TPU v7x, 32 devices: a whole 2x2x4 slice. The times are simulated.
32 devices in a mesh: sp: 8 (over z, x), tp: 4 (over y, core).
Axes of the slice: x: 2, y: 2, z: 4, core: 2. Of those that a mesh axis runs over, the one named last changes fastest.
Arguments:
- residual: bfloat16 [1024, 2048], P('sp', 'tp'), may hold values from -80 to 80
- query_wide: bfloat16 [1024, 1024], P('sp', 'tp'), may hold values from -6 to 6
- key_wide: bfloat16 [1024, 1024], P('sp', 'tp'), may hold values from -6 to 6
- query_narrow: bfloat16 [1024, 512], P('sp', 'tp'), may hold values from -6 to 6
- key_narrow: bfloat16 [1024, 512], P('sp', 'tp'), may hold values from -6 to 6
- values: bfloat16 [1024, 2048], P('sp', 'tp'), may hold values from -6 to 6
- gate_logits: float32 [4, 8, 1024], P(None, 'tp', 'sp'), may hold values from -6 to 106
- head_gain: float32 [2048], P('tp'), may hold values from 0.1 to 1.9
- norm_gain: float32 [2048], replicated, may hold values from 0.1 to 1.9
- route_experts: int32 [1024, 2], P('sp'), may hold values from 0 to 7, all different within a row; in each aligned block of 128 rows (0 to 127, 128 to 255, ...) at most 64 rows name the same one
- route_weights: float32 [1024, 2], P('sp'), may hold values from 0.2 to 1
- expert_gate: bfloat16 [8, 2048, 3584], P('sp', None, 'tp'), may hold values from -0.125 to 0.125
- expert_up: bfloat16 [8, 2048, 3584], P('sp', None, 'tp'), may hold values from -0.125 to 0.125
- expert_down: bfloat16 [8, 3584, 2048], P('sp', 'tp'), may hold values from -0.09375 to 0.09375
Outputs:
- layer_out: bfloat16 [1024, 2048], P('sp', 'tp')
Inputs may be any that keep to these rules, and one draw needn't show every extreme that they name: `route_experts`: each row names 2 different experts; within the rows of one device (aligned blocks of 128 rows) no expert is named more than 64 times, a bound that some block reaches.
All inputs are finite; a program needn't handle non-finite values.
Results may differ from a plain program's by a relative error of at most 0.0055.
Values may be sent and summed in bfloat16 or wider, within the bound.
A program may use at most 128 MiB of HBM per device.

v0:
```python
import functools

import jax
import jax.numpy as jnp
from jax import lax
from jax.experimental import pallas as pl
from jax.experimental.pallas import tpu as pltpu
from jax.sharding import PartitionSpec as P

precise = lax.Precision.HIGHEST
norm_eps = 1e-06


def prefix(part, axis, combine, identity, reverse):
    count = lax.axis_size(axis)
    place = lax.axis_index(axis)
    ahead = count - 1 - place if reverse else place
    gathered = jax.tree.map(lambda a: lax.all_gather(a, axis), part)
    state = jax.tree.map(lambda a, e: jnp.zeros_like(a) + jnp.asarray(e, a.dtype), part, identity)

    def one(step, state):
        source = count - 1 - step if reverse else step
        return combine(
            state, jax.tree.map(lambda a: lax.dynamic_index_in_dim(a, source, 0, False), gathered)
        )

    return lax.fori_loop(0, ahead, one, state)


def summarize(inputs):
    query_heads, key_heads, value_heads, log_in, log_keep = inputs
    running = jnp.cumsum(log_keep, axis=-1)
    total_log = running[:, -1]
    later_log = total_log[:, None] - running + log_in
    highest = jnp.max(later_log, axis=-1)
    weighted = key_heads * jnp.exp(later_log - highest[:, None])[..., None]
    memory = jnp.einsum("hsd,hse->hde", weighted, value_heads, precision=precise)
    return (memory, jnp.sum(weighted, axis=1), highest, total_log)


def empty_state(template):
    memory, normer, stabilizer, total_log = template
    return (
        jnp.zeros_like(memory),
        jnp.zeros_like(normer),
        jnp.full_like(stabilizer, -1e30),
        jnp.zeros_like(total_log),
    )


def join_states(earlier, later):
    joined = []
    for offset in range(0, len(earlier), 4):
        mem_old, norm_old, stab_old, total_old = earlier[offset : offset + 4]
        mem_new, norm_new, stab_new, total_new = later[offset : offset + 4]
        highest = jnp.maximum(stab_old + total_new, stab_new)
        old_scale = jnp.exp(stab_old + total_new - highest)
        new_scale = jnp.exp(stab_new - highest)
        joined += [
            old_scale[:, None, None] * mem_old + new_scale[:, None, None] * mem_new,
            old_scale[:, None] * norm_old + new_scale[:, None] * norm_new,
            highest,
            total_old + total_new,
        ]
    return tuple(joined)


def log_table(inputs):
    query_heads, key_heads, value_heads, log_in, log_keep = inputs
    running = jnp.cumsum(log_keep, axis=-1)
    positions = jnp.arange(running.shape[1])
    lower_mask = positions[:, None] >= positions[None, :]
    log_weights = jnp.where(
        lower_mask[None], running[:, :, None] - running[:, None, :] + log_in[:, None, :], -jnp.inf
    )
    scores = jnp.einsum("hld,hsd->hls", query_heads, key_heads, precision=precise)
    return (running, log_weights, scores)


def full_pass(inputs, carried):
    query_heads, value_heads = (inputs[0], inputs[2])
    memory, normer, stabilizer, total_log = carried
    running, log_weights, scores = log_table(inputs)
    carry_log = running + stabilizer[:, None]
    highest = jnp.maximum(carry_log, jnp.max(log_weights, axis=-1))
    carry_w = jnp.exp(carry_log - highest)
    intra_w = jnp.exp(log_weights - highest[:, :, None]) * scores
    numerator = carry_w[..., None] * jnp.einsum(
        "hld,hde->hle", query_heads, memory, precision=precise
    )
    numerator = numerator + jnp.einsum("hls,hse->hle", intra_w, value_heads, precision=precise)
    divisor = carry_w * jnp.einsum("hld,hd->hl", query_heads, normer, precision=precise) + jnp.sum(
        intra_w, axis=-1
    )
    return numerator / jnp.maximum(jnp.abs(divisor), jnp.exp(-highest))[..., None]


def body(
    residual,
    query_wide,
    key_wide,
    query_narrow,
    key_narrow,
    values,
    gate_logits,
    head_gain,
    norm_gain,
    route_experts,
    route_weights,
    expert_gate,
    expert_up,
    expert_down,
):
    heads_here = gate_logits.shape[1] // 2
    tok_rows = residual.shape[0]
    value_width = values.shape[1] // (2 * heads_here)
    value_all = values.astype(jnp.float32).reshape(tok_rows, heads_here, 2, value_width)
    groups = []
    for group_index, (query_in, key_in) in enumerate(
        ((query_wide, key_wide), (query_narrow, key_narrow))
    ):
        key_width = query_in.shape[1] // heads_here
        query_heads = (
            query_in.astype(jnp.float32).reshape(tok_rows, heads_here, key_width).transpose(1, 0, 2)
        )
        key_heads = key_in.astype(jnp.float32).reshape(tok_rows, heads_here, key_width).transpose(
            1, 0, 2
        ) * key_width ** (-0.5)
        value_heads = value_all[:, :, group_index].transpose(1, 0, 2)
        gates_here = gate_logits[:, group_index::2]
        ahead = (
            query_heads,
            key_heads,
            value_heads,
            gates_here[0],
            jax.nn.log_sigmoid(gates_here[1]),
        )
        behind = tuple(
            (
                jnp.flip(array, axis=1)
                for array in (
                    query_heads,
                    key_heads,
                    value_heads,
                    gates_here[2],
                    jax.nn.log_sigmoid(gates_here[3]),
                )
            )
        )
        groups.append((ahead, behind))
    forward_local = summarize(groups[0][0]) + summarize(groups[1][0])
    backward_local = summarize(groups[0][1]) + summarize(groups[1][1])
    forward_in = prefix(
        forward_local,
        "sp",
        join_states,
        empty_state(forward_local[:4]) + empty_state(forward_local[4:]),
        False,
    )
    backward_in = prefix(
        backward_local,
        "sp",
        join_states,
        empty_state(backward_local[:4]) + empty_state(backward_local[4:]),
        True,
    )
    cells = []
    for group_index, pair in enumerate(groups):
        halves = []
        for side, inputs in enumerate(pair):
            carried = (forward_in, backward_in)[side][4 * group_index : 4 * group_index + 4]
            output = full_pass(inputs, carried)
            if side == 1:
                output = jnp.flip(output, axis=1)
            halves.append(output)
        cells.append(halves[0] + halves[1])
    stacked = jnp.stack(cells, axis=1)
    stacked = stacked * lax.rsqrt(jnp.mean(stacked * stacked, axis=-1, keepdims=True) + norm_eps)
    stacked = stacked * head_gain.reshape(heads_here, 2, 1, value_width)
    heads_out = stacked.transpose(2, 0, 1, 3).reshape(tok_rows, -1)
    merged = (residual.astype(jnp.float32) + heads_out).astype(jnp.bfloat16)
    merged_f = merged.astype(jnp.float32)
    expert_total = lax.axis_size("sp")
    top_count = route_experts.shape[1]
    capacity = 2 * top_count * tok_rows // expert_total
    picks = route_experts.reshape(-1)
    pick_count = picks.shape[0]
    onehot = (picks[:, None] == jnp.arange(expert_total, dtype=jnp.int32)[None, :]).astype(
        jnp.int32
    )
    before = jnp.cumsum(onehot, axis=0) - onehot
    ranking = jnp.sum(before * onehot, axis=1)
    slot_of = picks * capacity + ranking
    owner = jnp.arange(pick_count, dtype=jnp.int32) // top_count
    source_row = jnp.zeros((expert_total * capacity,), jnp.int32).at[slot_of].set(owner)
    filled = jnp.zeros((expert_total * capacity,), jnp.bool_).at[slot_of].set(True)
    squares = lax.psum(jnp.sum(merged_f * merged_f, axis=1), "tp")
    own_width = merged.shape[1]
    gain_part = lax.dynamic_slice_in_dim(norm_gain, lax.axis_index("tp") * own_width, own_width)
    scale_row = lax.rsqrt(squares / (own_width * lax.axis_size("tp")) + norm_eps)
    normed = (merged_f * scale_row[:, None] * gain_part).astype(jnp.bfloat16)
    zero_row = jnp.zeros((), jnp.bfloat16)
    gathered = lax.all_gather(
        lax.all_to_all(
            jnp.where(filled[:, None], normed[source_row], zero_row).reshape(
                expert_total, capacity, -1
            ),
            "sp",
            split_axis=0,
            concat_axis=0,
            tiled=True,
        ),
        "tp",
        axis=2,
        tiled=True,
    )
    sources, slots, width_all = gathered.shape
    flat_rows = gathered.reshape(sources * slots, width_all)
    gate_proj = jnp.dot(flat_rows, expert_gate[0], preferred_element_type=jnp.float32)
    up_proj = jnp.dot(flat_rows, expert_up[0], preferred_element_type=jnp.float32)
    hidden = (jax.nn.silu(gate_proj) * up_proj).astype(jnp.bfloat16)
    partial_value = jnp.dot(hidden, expert_down[0], preferred_element_type=jnp.float32)
    summed = lax.psum_scatter(
        partial_value.astype(jnp.bfloat16), "tp", scatter_dimension=1, tiled=True
    )
    back = summed.reshape(sources, slots, -1)
    returned = lax.all_to_all(back, "sp", split_axis=0, concat_axis=0, tiled=True)
    flat_back = returned.reshape(expert_total * capacity, -1).astype(jnp.float32)
    picked = flat_back[slot_of] * route_weights.reshape(-1)[:, None]
    added = jnp.sum(picked.reshape(tok_rows, top_count, -1), axis=1)
    return (merged_f + added).astype(jnp.bfloat16)


MESH = pl.DeviceIdType.MESH
FAR = -1e30


def log_sigmoid(x):
    return jnp.minimum(x, 0.0) - jnp.log1p(jnp.exp(-jnp.abs(x)))


def layer_kernel(
    n,
    groups,
    pieces,
    heads_here,
    residual,
    query_wide,
    key_wide,
    query_narrow,
    key_narrow,
    values,
    gates,
    head_gain,
    norm_gain,
    route_experts,
    route_weights,
    gate_hbm,
    up_hbm,
    down_hbm,
    out,
    gates_all,
    key_wide_all,
    key_narrow_all,
    values_all,
    col_weight,
    acc,
    den,
    squares,
    slots_out,
    rows_in,
    lhs,
    partial_out,
    sib_in,
    pair_sum,
    cross_in,
    final,
    back,
    gate_w,
    up_w,
    down_w,
    weight_sem,
    gate_send,
    gate_recv,
    kv_send,
    kv_recv,
    sq_send,
    sq_recv,
    row_send,
    row_recv,
    sib_send,
    sib_recv,
    cross_send,
    cross_recv,
    back_send,
    back_recv,
):
    me = lax.axis_index("sp")
    col = lax.axis_index("tp")
    n_tp = lax.axis_size("tp")
    stations = n // 2
    station = me // 2
    side = me % 2
    pair = station * 2 + (1 - side)
    sib = (col // 2) * 2 + (1 - col % 2)
    cross = (col + 2) % n_tp
    cross_sib = (sib + 2) % n_tp
    rows, width = residual.shape
    cap = slots_out.shape[1]
    per_group = n // groups
    group_rows = per_group * cap
    head_count = 2 * heads_here
    dv = width // head_count

    fetch = [
        pltpu.make_async_copy(src.at[0], dst, weight_sem.at[i])
        for i, (src, dst) in enumerate(((gate_hbm, gate_w), (up_hbm, up_w), (down_hbm, down_w)))
    ]
    for copy in fetch:
        copy.start()

    barrier = pltpu.get_barrier_semaphore()
    for k in range(1, n):
        pl.semaphore_signal(
            barrier, inc=1, device_id=((me + k) % n, col), device_id_type=MESH
        )
    for k in range(1, n_tp):
        pl.semaphore_signal(
            barrier, inc=1, device_id=(me, (col + k) % n_tp), device_id_type=MESH
        )
    pl.semaphore_wait(barrier, n - 1 + n_tp - 1)

    def remote(src, dst, send, recv, sp, tp):
        return pltpu.make_async_remote_copy(
            src_ref=src,
            dst_ref=dst,
            send_sem=send,
            recv_sem=recv,
            device_id=(sp, tp),
            device_id_type=MESH,
        )

    def gate_copy(k, source):
        return remote(
            gates,
            gates_all.at[source],
            gate_send.at[k],
            gate_recv.at[source],
            (me + k) % n,
            col,
        )

    for k in range(1, n):
        gate_copy(k, me).start()

    streams = ((key_wide, key_wide_all), (key_narrow, key_narrow_all), (values, values_all))

    def kv_copies(kind, block, own, target):
        return [
            remote(
                local if own else whole.at[block],
                whole.at[block],
                kv_send.at[kind, a, block],
                kv_recv.at[a, block],
                target,
                col,
            )
            for a, (local, whole) in enumerate(streams)
        ]

    def each(copies, act):
        for copy in copies:
            getattr(copy, act)()

    up_there = station < stations - 1
    down_there = station > 0

    @pl.when(up_there)
    def _():
        each(kv_copies(1, me, True, me + 2), "start")

    @pl.when(down_there)
    def _():
        each(kv_copies(2, me, True, me - 2), "start")

    each(kv_copies(0, me, True, pair), "start")

    gates_all[me] = gates[...]
    for k in range(1, n):
        gate_copy(k, (me - k + n) % n).wait_recv()

    t_iota = lax.broadcasted_iota(jnp.int32, (rows, rows), 0)
    s_iota = lax.broadcasted_iota(jnp.int32, (rows, rows), 1)
    lower = (t_iota >= s_iota).astype(jnp.float32)
    upper = (t_iota <= s_iota).astype(jnp.float32)
    strict_low = (t_iota > s_iota).astype(jnp.float32)
    strict_up = (t_iota < s_iota).astype(jnp.float32)
    exact = functools.partial(
        jnp.dot, precision=precise, preferred_element_type=jnp.float32
    )
    n_iota = lax.broadcasted_iota(jnp.int32, (n, rows), 0)

    queries = []
    for h in range(head_count):
        j, g = h // 2, h % 2
        q_ref, k_ref, k_all = (
            (query_wide, key_wide, key_wide_all),
            (query_narrow, key_narrow, key_narrow_all),
        )[g]
        dk = q_ref.shape[1] // heads_here
        queries.append((q_ref, k_ref, k_all, j * dk, dk))

    def scores_of(h, keys):
        q_ref, _, _, start, dk = queries[h]
        return lax.dot_general(
            q_ref[:, start : start + dk],
            keys,
            (((1,), (1,)), ((), ())),
            preferred_element_type=jnp.float32,
        ) * (dk ** (-0.5))

    def weighted_values(weights, vals):
        high = weights.astype(jnp.bfloat16)
        low = (weights - high.astype(jnp.float32)).astype(jnp.bfloat16)
        return jnp.dot(high, vals, preferred_element_type=jnp.float32) + jnp.dot(
            low, vals, preferred_element_type=jnp.float32
        )

    def row_of(plane, h):
        return plane * head_count + h

    own_parts = []
    for h in range(head_count):
        own_scores = scores_of(
            h, queries[h][1][:, queries[h][3] : queries[h][3] + queries[h][4]]
        )
        own_values = values[:, h * dv : (h + 1) * dv]
        halves = []
        for d in range(2):
            keep = log_sigmoid(gates_all[:, row_of(2 * d + 1, h), :])
            log_in = gates_all[:, row_of(2 * d, h), :]
            later = exact(keep, strict_low if d == 0 else strict_up) + log_in
            totals = jnp.sum(keep, axis=1, keepdims=True)
            between = jnp.zeros((n, rows), jnp.float32)
            for i in range(n):
                if d == 0:
                    inside = (n_iota < i) & (i < me)
                else:
                    inside = (n_iota > i) & (i > me)
                between = between + jnp.where(inside, totals[i : i + 1, :], 0.0)
            beyond = (n_iota < me) if d == 0 else (n_iota > me)
            later = jnp.where(beyond, later + between, FAR)
            top = jnp.max(jnp.max(later, axis=1, keepdims=True), axis=0, keepdims=True)
            col_weight[d, h] = jnp.where(beyond, jnp.exp(later - top), 0.0)
            keep_row = log_sigmoid(gates[row_of(2 * d + 1, h) : row_of(2 * d + 1, h) + 1, :])
            in_row = gates[row_of(2 * d, h) : row_of(2 * d, h) + 1, :]
            mask = lower if d == 0 else upper
            run_col = jnp.sum(mask * keep_row, axis=1, keepdims=True)
            keep_rows = jnp.broadcast_to(keep_row, (8, rows))
            run_row = exact(keep_rows, upper if d == 0 else lower)[0:1, :]
            logs = jnp.where(mask > 0.5, run_col - run_row + in_row, FAR)
            highest = jnp.maximum(jnp.max(logs, axis=1, keepdims=True), run_col + top)
            carry = jnp.exp(run_col + top - highest)
            weights = jnp.exp(logs - highest) * own_scores
            halves.append(
                (
                    weighted_values(weights, own_values),
                    jnp.sum(weights, axis=1, keepdims=True),
                    highest,
                    carry,
                )
            )
        own_parts.append(halves)
    acc[...] = jnp.zeros_like(acc)
    den[...] = jnp.zeros_like(den)

    def process(block):
        d = (block > me).astype(jnp.int32)
        for h in range(head_count):
            _, _, k_all, start, dk = queries[h]
            s = scores_of(h, k_all[block, :, start : start + dk])
            weights = s * col_weight[d, h, pl.ds(block, 1), :]
            vals = values_all[block, :, h * dv : (h + 1) * dv]
            acc[d, h] += weighted_values(weights, vals)
            den[d, h] += weights

    def arrive(kind, block, there, target):
        each(kv_copies(kind, block, False, pair), "wait_recv")

        @pl.when(there)
        def _():
            each(kv_copies(kind, block, False, target), "start")

        each(kv_copies(0, block, False, pair), "start")

    def from_pair(block):
        each(kv_copies(0, block, False, pair), "wait_recv")
        process(block)

    def step(d, carry):
        low_ok, high_ok = station - d >= 0, station + d < stations
        low, high = me - 2 * d, me + 2 * d

        @pl.when(low_ok)
        def _():
            arrive(1, low, up_there, me + 2)

        @pl.when(high_ok)
        def _():
            arrive(2, high, down_there, me - 2)

        @pl.when(low_ok)
        def _():
            process(low)

        @pl.when(high_ok)
        def _():
            process(high)

        @pl.when(station - (d - 1) >= 0)
        def _():
            from_pair(pair - 2 * (d - 1))

        @pl.when((station + (d - 1) < stations) & (d > 1))
        def _():
            from_pair(pair + 2 * (d - 1))

        return carry

    lax.fori_loop(1, stations, step, 0)
    last = stations - 1

    @pl.when(station - last >= 0)
    def _():
        from_pair(pair - 2 * last)

    if last > 0:

        @pl.when(station + last < stations)
        def _():
            from_pair(pair + 2 * last)

    square_row = jnp.zeros((8, rows), jnp.float32)
    merged_parts = []
    for h in range(head_count):
        total = None
        for d in range(2):
            own_num, own_den, highest, carry = own_parts[h][d]
            num = carry * acc[d, h] + own_num
            div = carry * jnp.sum(den[d, h], axis=1, keepdims=True) + own_den
            part = num / jnp.maximum(jnp.abs(div), jnp.exp(-highest))
            total = part if total is None else total + part
        total = total * lax.rsqrt(jnp.mean(total * total, axis=1, keepdims=True) + norm_eps)
        total = total * head_gain[:, h * dv : (h + 1) * dv]
        cut = slice(h * dv, (h + 1) * dv)
        merged = (residual[:, cut].astype(jnp.float32) + total).astype(jnp.bfloat16)
        merged_parts.append(merged)
        merged_f = merged.astype(jnp.float32)
        square_row = square_row + lax.dot_general(
            jnp.ones((8, dv), jnp.float32),
            merged_f * merged_f,
            (((1,), (1,)), ((), ())),
            precision=precise,
            preferred_element_type=jnp.float32,
        )
    squares[col] = square_row

    def sq_copy(k, source):
        return remote(
            squares.at[source],
            squares.at[source],
            sq_send.at[k],
            sq_recv.at[source],
            me,
            (col + k) % n_tp,
        )

    for k in range(1, n_tp):
        sq_copy(k, col).start()

    lane = lax.broadcasted_iota(jnp.int32, (rows, rows), 1)
    def column_of(row):
        return jnp.sum(jnp.where(t_iota == s_iota, row, 0), axis=1, keepdims=True)

    picks = [
        column_of(route_experts[p : p + 1, :].astype(jnp.float32)).astype(jnp.int32)
        for p in range(route_experts.shape[0])
    ]
    mixes = [column_of(route_weights[p : p + 1, :]) for p in range(route_experts.shape[0])]
    named = jnp.zeros((rows, rows), jnp.float32)
    for pick in picks:
        named = named + (lane == pick).astype(jnp.float32)
    named = named.astype(jnp.bfloat16)
    rank = jnp.dot(strict_low.astype(jnp.bfloat16), named, preferred_element_type=jnp.float32)
    over_rows = (((0,), (0,)), ((), ()))
    rank_t = lax.dot_general(
        named, strict_up.astype(jnp.bfloat16), over_rows, preferred_element_type=jnp.float32
    )
    named_t = lax.dot_general(
        named,
        (t_iota == s_iota).astype(jnp.bfloat16),
        over_rows,
        preferred_element_type=jnp.float32,
    )
    rank_t = jnp.where(named_t > 0.5, rank_t, -1.0)
    slot_iota = lax.broadcasted_iota(jnp.int32, (cap, rows), 0).astype(jnp.float32)

    for k in range(1, n_tp):
        sq_copy(k, (col - k + n_tp) % n_tp).wait_recv()
    square_sum = squares[0, 0:1, :]
    for c in range(1, n_tp):
        square_sum = square_sum + squares[c, 0:1, :]
    square_col = jnp.sum(jnp.where(t_iota == s_iota, square_sum, 0.0), axis=1, keepdims=True)
    scale = lax.rsqrt(square_col / (width * n_tp) + norm_eps)
    merged = jnp.concatenate(merged_parts, axis=1)
    merged_f = merged.astype(jnp.float32)
    gain = norm_gain[:, pl.ds(pl.multiple_of(col * width, width), width)]
    normed = (merged_f * scale * gain).astype(jnp.bfloat16)

    for e in range(n):
        choose = (slot_iota == rank_t[e : e + 1, :]).astype(jnp.bfloat16)
        slots_out[e] = jnp.dot(choose, normed, preferred_element_type=jnp.float32).astype(
            jnp.bfloat16
        )

    offsets = [(k + 1) // 2 if k % 2 else (n - k // 2) % n for k in range(n)]

    def back_of(k):
        return (me - offsets[k] + n) % n

    def ahead_of(k):
        return (me + offsets[k]) % n

    def row_copy(kind, k):
        if kind == 0:
            return remote(
                slots_out.at[ahead_of(k)],
                rows_in.at[col, me],
                row_send.at[0, k],
                row_recv.at[0, k],
                ahead_of(k),
                col,
            )
        source = back_of(k)
        column, target = ((col, cross), (col, sib), (cross, sib))[kind - 1]
        return remote(
            rows_in.at[column, source],
            rows_in.at[column, source],
            row_send.at[kind, k],
            row_recv.at[kind, k],
            me,
            target,
        )

    def row_arrival(kind, k):
        source = back_of(k)
        column = (col, cross, sib, cross_sib)[kind]
        return remote(
            rows_in.at[column, source],
            rows_in.at[column, source],
            row_send.at[kind, k],
            row_recv.at[kind, k],
            (me + k) % n,
            sib,
        )

    for k in range(1, n):
        row_copy(0, k).start()
    rows_in[col, me] = slots_out[me]

    def spread(g):
        ks = range(g * per_group, (g + 1) * per_group)
        for k in ks:
            if k > 0:
                row_arrival(0, k).wait_recv()
            row_copy(1, k).start()
            row_copy(2, k).start()

    def relay(g):
        for k in range(g * per_group, (g + 1) * per_group):
            row_arrival(1, k).wait_recv()
            row_copy(3, k).start()

    def expert(g):
        for k in range(g * per_group, (g + 1) * per_group):
            row_arrival(2, k).wait_recv()
            row_arrival(3, k).wait_recv()
        for k in range(g * per_group, (g + 1) * per_group):
            at = (k - g * per_group) * cap
            for c in range(n_tp):
                lhs[at : at + cap, c * width : (c + 1) * width] = rows_in[c, back_of(k)]
        if g == 0:
            for copy in fetch:
                copy.wait()
        features = lhs[...]
        gate_proj = jnp.dot(features, gate_w[...], preferred_element_type=jnp.float32)
        up_proj = jnp.dot(features, up_w[...], preferred_element_type=jnp.float32)
        hidden = (gate_proj * jax.nn.sigmoid(gate_proj) * up_proj).astype(jnp.bfloat16)
        for i, c in enumerate((cross_sib, cross, sib, col)):
            part = jnp.dot(
                hidden,
                down_w[:, pl.ds(pl.multiple_of(c * width, width), width)],
                preferred_element_type=jnp.float32,
            )
            partial_out[c, g] = part.astype(jnp.bfloat16)
            if i % 2 == 0:
                sib_copy(i // 2, g).start()

    def sib_copy(i, g):
        return remote(
            partial_out.at[(cross_sib, sib)[i], g],
            sib_in.at[i, g],
            sib_send.at[i, g],
            sib_recv.at[i, g],
            me,
            sib,
        )

    piece = group_rows // pieces

    def cross_copy(g, i):
        cut = slice(i * piece, (i + 1) * piece)
        return remote(
            pair_sum.at[g, cut],
            cross_in.at[g, cut],
            cross_send.at[g, i],
            cross_recv.at[g, i],
            me,
            cross,
        )

    def add_pair(g):
        sib_copy(0, g).wait_recv()
        for i in range(pieces):
            cut = slice(i * piece, (i + 1) * piece)
            pair_sum[g, cut] = (
                partial_out[cross, g, cut].astype(jnp.float32)
                + sib_in[0, g, cut].astype(jnp.float32)
            ).astype(jnp.bfloat16)
            cross_copy(g, i).start()

    def back_copy(k, arriving):
        g, at = k // per_group, (k % per_group) * cap
        expert_at = ahead_of(k) if arriving else me
        return remote(
            final.at[g, at : at + cap],
            back.at[expert_at],
            back_send.at[k],
            back_recv.at[k],
            back_of(k),
            col,
        )

    def finish(g):
        sib_copy(1, g).wait_recv()
        per_piece = per_group // pieces
        for i in range(pieces):
            cut = slice(i * piece, (i + 1) * piece)
            cross_copy(g, i).wait_recv()
            final[g, cut] = (
                partial_out[col, g, cut].astype(jnp.float32)
                + sib_in[1, g, cut].astype(jnp.float32)
                + cross_in[g, cut].astype(jnp.float32)
            ).astype(jnp.bfloat16)
            first = g * per_group + i * per_piece
            for k in range(first, first + per_piece):
                if k > 0:
                    back_copy(k, False).start()
        if g == 0:
            back[me] = final[0, 0:cap, :]

    spread(0)
    spread(1)
    relay(0)
    expert(0)
    for g in range(1, groups):
        if g + 1 < groups:
            spread(g + 1)
        add_pair(g - 1)
        relay(g)
        expert(g)
        finish(g - 1)
    add_pair(groups - 1)
    finish(groups - 1)

    wide_lane = lax.broadcasted_iota(jnp.int32, (rows, n * cap), 1)
    takes = []
    for pick in picks:
        place = jnp.sum(jnp.where(lane == pick, rank, 0.0), axis=1, keepdims=True)
        slot = pick * cap + place.astype(jnp.int32)
        takes.append((wide_lane == slot).astype(jnp.bfloat16))
    for k in range(1, n):
        back_copy(k, True).wait_recv()
    returned = back[...].reshape(n * cap, width)
    added = merged_f
    for p, take in enumerate(takes):
        added = added + mixes[p] * jnp.dot(
            take, returned, preferred_element_type=jnp.float32
        )
    out[...] = added.astype(jnp.bfloat16)

    for k in range(1, n):
        gate_copy(k, me).wait_send()
        row_copy(0, k).wait_send()
        back_copy(k, False).wait_send()
    for k in range(1, n_tp):
        sq_copy(k, col).wait_send()
    for k in range(n):
        for kind in (1, 2, 3):
            row_copy(kind, k).wait_send()
    for g in range(groups):
        sib_copy(0, g).wait_send()
        sib_copy(1, g).wait_send()
        for i in range(pieces):
            cross_copy(g, i).wait_send()

    each(kv_copies(0, me, False, pair), "wait_send")

    @pl.when(up_there)
    def _():
        each(kv_copies(1, me, False, me + 2), "wait_send")

    @pl.when(down_there)
    def _():
        each(kv_copies(2, me, False, me - 2), "wait_send")

    def drain(d, carry):
        @pl.when(station - d >= 0)
        def _():
            each(kv_copies(0, me - 2 * d, False, pair), "wait_send")

            @pl.when(up_there)
            def _():
                each(kv_copies(1, me - 2 * d, False, me + 2), "wait_send")

        @pl.when(station + d < stations)
        def _():
            each(kv_copies(0, me + 2 * d, False, pair), "wait_send")

            @pl.when(down_there)
            def _():
                each(kv_copies(2, me + 2 * d, False, me - 2), "wait_send")

        return carry

    lax.fori_loop(1, stations, drain, 0)


def layer(
    residual,
    query_wide,
    key_wide,
    query_narrow,
    key_narrow,
    values,
    gate_logits,
    head_gain,
    norm_gain,
    route_experts,
    route_weights,
    expert_gate,
    expert_up,
    expert_down,
    n,
    n_tp,
):
    rows, width = residual.shape
    head_count = gate_logits.shape[1]
    cap = 2 * route_experts.shape[1] * rows // n
    groups = 2
    pieces = 4
    group_rows = n // groups * cap
    dv = width // head_count
    bf, f32 = jnp.bfloat16, jnp.float32
    vmem = pl.BlockSpec(memory_space=pltpu.VMEM)
    hbm = pl.BlockSpec(memory_space=pl.ANY)
    dma = pltpu.SemaphoreType.DMA
    return pl.pallas_call(
        functools.partial(layer_kernel, n, groups, pieces, head_count // 2),
        out_shape=jax.ShapeDtypeStruct((rows, width), bf),
        in_specs=[vmem] * 11 + [hbm] * 3,
        out_specs=vmem,
        scratch_shapes=[
            pltpu.VMEM((n, 4 * head_count, rows), f32),
            pltpu.VMEM((n,) + key_wide.shape, bf),
            pltpu.VMEM((n,) + key_narrow.shape, bf),
            pltpu.VMEM((n,) + values.shape, bf),
            pltpu.VMEM((2, head_count, n, rows), f32),
            pltpu.VMEM((2, head_count, rows, dv), f32),
            pltpu.VMEM((2, head_count, rows, rows), f32),
            pltpu.VMEM((n_tp, 8, rows), f32),
            pltpu.VMEM((n, cap, width), bf),
            pltpu.VMEM((n_tp, n, cap, width), bf),
            pltpu.VMEM((group_rows, n_tp * width), bf),
            pltpu.VMEM((n_tp, groups, group_rows, width), bf),
            pltpu.VMEM((2, groups, group_rows, width), bf),
            pltpu.VMEM((groups, group_rows, width), bf),
            pltpu.VMEM((groups, group_rows, width), bf),
            pltpu.VMEM((groups, group_rows, width), bf),
            pltpu.VMEM((n, cap, width), bf),
            pltpu.VMEM(expert_gate.shape[1:], bf),
            pltpu.VMEM(expert_up.shape[1:], bf),
            pltpu.VMEM(expert_down.shape[1:], bf),
            dma((3,)),
            dma((n,)),
            dma((n,)),
            dma((3, 3, n)),
            dma((3, n)),
            dma((n_tp,)),
            dma((n_tp,)),
            dma((4, n)),
            dma((4, n)),
            dma((2, groups)),
            dma((2, groups)),
            dma((groups, pieces)),
            dma((groups, pieces)),
            dma((n,)),
            dma((n,)),
        ],
        compiler_params=pltpu.CompilerParams(
            collective_id=0, has_side_effects=True, vmem_limit_bytes=60 * 1024 * 1024
        ),
    )(
        residual,
        query_wide,
        key_wide,
        query_narrow,
        key_narrow,
        values,
        gate_logits.reshape(4 * head_count, rows),
        head_gain.reshape(1, -1),
        norm_gain.reshape(1, -1),
        route_experts.T,
        route_weights.T,
        expert_gate,
        expert_up,
        expert_down,
    )


def fits(n, n_tp, args):
    rows = args[0].shape[0]
    cap = 2 * args[9].shape[1] * rows // n
    return n_tp == 4 and n % 8 == 0 and n <= 128 and rows == 128 and cap % 16 == 0


def choose(n, n_tp, *args):
    if fits(n, n_tp, args):
        return layer(*args, n, n_tp)
    return body(*args)


def solution(mesh):
    return jax.shard_map(
        functools.partial(choose, mesh.shape["sp"], mesh.shape["tp"]),
        mesh=mesh,
        in_specs=(
            P("sp", "tp"),
            P("sp", "tp"),
            P("sp", "tp"),
            P("sp", "tp"),
            P("sp", "tp"),
            P("sp", "tp"),
            P(None, "tp", "sp"),
            P("tp"),
            P(),
            P("sp", None),
            P("sp", None),
            P("sp", None, "tp"),
            P("sp", None, "tp"),
            P("sp", "tp", None),
        ),
        out_specs=P("sp", "tp"),
        check_vma=False,
    )
```

profile of v0, /device:TPU:0, one launch (start us, length us, event | category | flops | bytes accessed | tf_op | source)
XLA Modules:
  0.0 78.1 jit_solution(9448772531697115932)
XLA Ops:
  0.0 76.5 %shard_map.136 = bf16[128,512]{1,0:T(8,128)(2,1)} custom-call(bf16[128,512]{1,0:T(8,128)(2,1)} %residual.1, bf16[128,256]{1,0:T(8,128)(2,1)} %query_wide.1, bf16[128,256]{1,0:T(8,128)(2,1)} %key_wide.1, bf16[128,128]{1,0:T(8,128)(2,1)} %query_narrow.1, bf16[128,128]{1,0:T(8,128)(2,1)} %key_narrow.1, bf16[128,512]{1,0:T(8,128)(2,1)} %values.1, ...), custom_call_target="tpu_custom_call" | custom-call | tf_op jit(solution)/shard_map/pallas_call | solution.py:878
  76.5 1.6 %copy.16 = bf16[128,512]{1,0:T(8,128)(2,1)} copy(bf16[128,512]{1,0:T(8,128)(2,1)} %shard_map.136) | data formatting | bytes 262144
where the time goes:
time: 78.3 us; the launch traced here: 78.1 us
  Pallas kernels  76.5 us (98%)
  local copies, waits for them, and re-layouts  1.57 us (2%)
    pallas_call x1, Pallas kernels, layer(): pl.pallas_call(functools.partial(layer_kernel, n, groups, pieces, head_co...  76.5 us
    unnamed x1, local copies, waits for them, and re-layouts  1.57 us

commit v1 on v0

--- a/solution.py
+++ b/solution.py
@@ -244,57 +244,63 @@
     groups,
     pieces,
     heads_here,
-    residual,
-    query_wide,
-    key_wide,
-    query_narrow,
-    key_narrow,
-    values,
-    gates,
-    head_gain,
-    norm_gain,
-    route_experts,
-    route_weights,
-    gate_hbm,
-    up_hbm,
-    down_hbm,
-    out,
-    gates_all,
-    key_wide_all,
-    key_narrow_all,
-    values_all,
-    col_weight,
-    acc,
-    den,
-    squares,
-    slots_out,
-    rows_in,
-    lhs,
-    partial_out,
-    sib_in,
-    pair_sum,
-    cross_in,
-    final,
-    back,
-    gate_w,
-    up_w,
-    down_w,
-    weight_sem,
-    gate_send,
-    gate_recv,
-    kv_send,
-    kv_recv,
-    sq_send,
-    sq_recv,
-    row_send,
-    row_recv,
-    sib_send,
-    sib_recv,
-    cross_send,
-    cross_recv,
-    back_send,
-    back_recv,
+    *refs,
 ):
+    small_count = 11
+    sources = refs[:small_count]
+    gate_hbm, up_hbm, down_hbm, out = refs[small_count : small_count + 4]
+    held = refs[small_count + 4 : 2 * small_count + 4]
+    (
+        residual,
+        query_wide,
+        key_wide,
+        query_narrow,
+        key_narrow,
+        values,
+        gates,
+        head_gain,
+        norm_gain,
+        route_experts,
+        route_weights,
+    ) = held
+    (
+        gates_all,
+        key_wide_all,
+        key_narrow_all,
+        values_all,
+        col_weight,
+        acc,
+        den,
+        slots_out,
+        rows_in,
+        lhs,
+        hidden,
+        partial_out,
+        sib_in,
+        pair_sum,
+        cross_in,
+        final,
+        back,
+        gate_w,
+        up_w,
+        down_w,
+        out_held,
+        weight_sem,
+        small_sem,
+        out_sem,
+        gate_send,
+        gate_recv,
+        kv_send,
+        kv_recv,
+        row_send,
+        row_recv,
+        sib_send,
+        sib_recv,
+        cross_send,
+        cross_recv,
+        back_send,
+        back_recv,
+    ) = refs[2 * small_count + 4 :]
     me = lax.axis_index("sp")
     col = lax.axis_index("tp")
     n_tp = lax.axis_size("tp")
@@ -312,6 +318,21 @@
     head_count = 2 * heads_here
     dv = width // head_count
 
+    barrier = pltpu.get_barrier_semaphore()
+    for k in range(1, n):
+        pl.semaphore_signal(
+            barrier, inc=1, device_id=((me + k) % n, col), device_id_type=MESH
+        )
+    for k in range(1, n_tp):
+        pl.semaphore_signal(
+            barrier, inc=1, device_id=(me, (col + k) % n_tp), device_id_type=MESH
+        )
+    load = [
+        pltpu.make_async_copy(src, dst, small_sem.at[i])
+        for i, (src, dst) in enumerate(zip(sources, held))
+    ]
+    for i in (6, 2, 4, 5, 1, 3, 0, 7, 8, 9, 10):
+        load[i].start()
     fetch = [
         pltpu.make_async_copy(src.at[0], dst, weight_sem.at[i])
         for i, (src, dst) in enumerate(((gate_hbm, gate_w), (up_hbm, up_w), (down_hbm, down_w)))
@@ -319,15 +340,8 @@
     for copy in fetch:
         copy.start()
 
-    barrier = pltpu.get_barrier_semaphore()
-    for k in range(1, n):
-        pl.semaphore_signal(
-            barrier, inc=1, device_id=((me + k) % n, col), device_id_type=MESH
-        )
-    for k in range(1, n_tp):
-        pl.semaphore_signal(
-            barrier, inc=1, device_id=(me, (col + k) % n_tp), device_id_type=MESH
-        )
+    for copy in load:
+        copy.wait()
     pl.semaphore_wait(barrier, n - 1 + n_tp - 1)
 
     def remote(src, dst, send, recv, sp, tp):
@@ -540,7 +554,6 @@
         def _():
             from_pair(pair + 2 * last)
 
-    square_row = jnp.zeros((8, rows), jnp.float32)
     merged_parts = []
     for h in range(head_count):
         total = None
@@ -555,28 +568,6 @@
         cut = slice(h * dv, (h + 1) * dv)
         merged = (residual[:, cut].astype(jnp.float32) + total).astype(jnp.bfloat16)
         merged_parts.append(merged)
-        merged_f = merged.astype(jnp.float32)
-        square_row = square_row + lax.dot_general(
-            jnp.ones((8, dv), jnp.float32),
-            merged_f * merged_f,
-            (((1,), (1,)), ((), ())),
-            precision=precise,
-            preferred_element_type=jnp.float32,
-        )
-    squares[col] = square_row
-
-    def sq_copy(k, source):
-        return remote(
-            squares.at[source],
-            squares.at[source],
-            sq_send.at[k],
-            sq_recv.at[source],
-            me,
-            (col + k) % n_tp,
-        )
-
-    for k in range(1, n_tp):
-        sq_copy(k, col).start()
 
     lane = lax.broadcasted_iota(jnp.int32, (rows, rows), 1)
     def column_of(row):
@@ -605,21 +596,11 @@
     rank_t = jnp.where(named_t > 0.5, rank_t, -1.0)
     slot_iota = lax.broadcasted_iota(jnp.int32, (cap, rows), 0).astype(jnp.float32)
 
-    for k in range(1, n_tp):
-        sq_copy(k, (col - k + n_tp) % n_tp).wait_recv()
-    square_sum = squares[0, 0:1, :]
-    for c in range(1, n_tp):
-        square_sum = square_sum + squares[c, 0:1, :]
-    square_col = jnp.sum(jnp.where(t_iota == s_iota, square_sum, 0.0), axis=1, keepdims=True)
-    scale = lax.rsqrt(square_col / (width * n_tp) + norm_eps)
     merged = jnp.concatenate(merged_parts, axis=1)
     merged_f = merged.astype(jnp.float32)
-    gain = norm_gain[:, pl.ds(pl.multiple_of(col * width, width), width)]
-    normed = (merged_f * scale * gain).astype(jnp.bfloat16)
-
     for e in range(n):
         choose = (slot_iota == rank_t[e : e + 1, :]).astype(jnp.bfloat16)
-        slots_out[e] = jnp.dot(choose, normed, preferred_element_type=jnp.float32).astype(
+        slots_out[e] = jnp.dot(choose, merged, preferred_element_type=jnp.float32).astype(
             jnp.bfloat16
         )
 
@@ -668,37 +649,46 @@
         row_copy(0, k).start()
     rows_in[col, me] = slots_out[me]
 
-    def spread(g):
-        ks = range(g * per_group, (g + 1) * per_group)
+    def spread(ks):
         for k in ks:
             if k > 0:
                 row_arrival(0, k).wait_recv()
             row_copy(1, k).start()
             row_copy(2, k).start()
 
-    def relay(g):
-        for k in range(g * per_group, (g + 1) * per_group):
+    def relay(ks):
+        for k in ks:
             row_arrival(1, k).wait_recv()
             row_copy(3, k).start()
 
-    def expert(g):
-        for k in range(g * per_group, (g + 1) * per_group):
+    def members(g):
+        return range(g * per_group, (g + 1) * per_group)
+
+    def prepare(g):
+        for k in members(g):
             row_arrival(2, k).wait_recv()
             row_arrival(3, k).wait_recv()
-        for k in range(g * per_group, (g + 1) * per_group):
             at = (k - g * per_group) * cap
-            for c in range(n_tp):
-                lhs[at : at + cap, c * width : (c + 1) * width] = rows_in[c, back_of(k)]
+            parts = [rows_in[c, back_of(k)].astype(jnp.float32) for c in range(n_tp)]
+            square = sum(jnp.sum(part * part, axis=1, keepdims=True) for part in parts)
+            scale = lax.rsqrt(square / (width * n_tp) + norm_eps)
+            for c, part in enumerate(parts):
+                cut = slice(c * width, (c + 1) * width)
+                lhs[at : at + cap, cut] = (part * scale * norm_gain[:, cut]).astype(jnp.bfloat16)
+
+    def gate_up(g):
         if g == 0:
             for copy in fetch:
                 copy.wait()
         features = lhs[...]
         gate_proj = jnp.dot(features, gate_w[...], preferred_element_type=jnp.float32)
         up_proj = jnp.dot(features, up_w[...], preferred_element_type=jnp.float32)
-        hidden = (gate_proj * jax.nn.sigmoid(gate_proj) * up_proj).astype(jnp.bfloat16)
+        hidden[...] = (gate_proj * jax.nn.sigmoid(gate_proj) * up_proj).astype(jnp.bfloat16)
+
+    def down(g):
         for i, c in enumerate((cross_sib, cross, sib, col)):
             part = jnp.dot(
-                hidden,
+                hidden[...],
                 down_w[:, pl.ds(pl.multiple_of(c * width, width), width)],
                 preferred_element_type=jnp.float32,
             )
@@ -769,19 +759,23 @@
         if g == 0:
             back[me] = final[0, 0:cap, :]
 
-    spread(0)
-    spread(1)
-    relay(0)
-    expert(0)
-    for g in range(1, groups):
-        if g + 1 < groups:
-            spread(g + 1)
-        add_pair(g - 1)
-        relay(g)
-        expert(g)
-        finish(g - 1)
-    add_pair(groups - 1)
-    finish(groups - 1)
+    late = members(1)
+    half = per_group // 2
+    spread(members(0))
+    spread(late[:half])
+    relay(members(0))
+    prepare(0)
+    gate_up(0)
+    spread(late[half:])
+    down(0)
+    add_pair(0)
+    relay(late)
+    prepare(1)
+    gate_up(1)
+    down(1)
+    add_pair(1)
+    finish(0)
+    finish(1)
 
     wide_lane = lax.broadcasted_iota(jnp.int32, (rows, n * cap), 1)
     takes = []
@@ -797,14 +791,14 @@
         added = added + mixes[p] * jnp.dot(
             take, returned, preferred_element_type=jnp.float32
         )
-    out[...] = added.astype(jnp.bfloat16)
+    out_held[...] = added.astype(jnp.bfloat16)
+    store = pltpu.make_async_copy(out_held, out, out_sem)
+    store.start()
 
     for k in range(1, n):
         gate_copy(k, me).wait_send()
         row_copy(0, k).wait_send()
         back_copy(k, False).wait_send()
-    for k in range(1, n_tp):
-        sq_copy(k, col).wait_send()
     for k in range(n):
         for kind in (1, 2, 3):
             row_copy(kind, k).wait_send()
@@ -844,6 +838,7 @@
         return carry
 
     lax.fori_loop(1, stations, drain, 0)
+    store.wait()
 
 
 def layer(
@@ -872,55 +867,7 @@
     group_rows = n // groups * cap
     dv = width // head_count
     bf, f32 = jnp.bfloat16, jnp.float32
-    vmem = pl.BlockSpec(memory_space=pltpu.VMEM)
-    hbm = pl.BlockSpec(memory_space=pl.ANY)
-    dma = pltpu.SemaphoreType.DMA
-    return pl.pallas_call(
-        functools.partial(layer_kernel, n, groups, pieces, head_count // 2),
-        out_shape=jax.ShapeDtypeStruct((rows, width), bf),
-        in_specs=[vmem] * 11 + [hbm] * 3,
-        out_specs=vmem,
-        scratch_shapes=[
-            pltpu.VMEM((n, 4 * head_count, rows), f32),
-            pltpu.VMEM((n,) + key_wide.shape, bf),
-            pltpu.VMEM((n,) + key_narrow.shape, bf),
-            pltpu.VMEM((n,) + values.shape, bf),
-            pltpu.VMEM((2, head_count, n, rows), f32),
-            pltpu.VMEM((2, head_count, rows, dv), f32),
-            pltpu.VMEM((2, head_count, rows, rows), f32),
-            pltpu.VMEM((n_tp, 8, rows), f32),
-            pltpu.VMEM((n, cap, width), bf),
-            pltpu.VMEM((n_tp, n, cap, width), bf),
-            pltpu.VMEM((group_rows, n_tp * width), bf),
-            pltpu.VMEM((n_tp, groups, group_rows, width), bf),
-            pltpu.VMEM((2, groups, group_rows, width), bf),
-            pltpu.VMEM((groups, group_rows, width), bf),
-            pltpu.VMEM((groups, group_rows, width), bf),
-            pltpu.VMEM((groups, group_rows, width), bf),
-            pltpu.VMEM((n, cap, width), bf),
-            pltpu.VMEM(expert_gate.shape[1:], bf),
-            pltpu.VMEM(expert_up.shape[1:], bf),
-            pltpu.VMEM(expert_down.shape[1:], bf),
-            dma((3,)),
-            dma((n,)),
-            dma((n,)),
-            dma((3, 3, n)),
-            dma((3, n)),
-            dma((n_tp,)),
-            dma((n_tp,)),
-            dma((4, n)),
-            dma((4, n)),
-            dma((2, groups)),
-            dma((2, groups)),
-            dma((groups, pieces)),
-            dma((groups, pieces)),
-            dma((n,)),
-            dma((n,)),
-        ],
-        compiler_params=pltpu.CompilerParams(
-            collective_id=0, has_side_effects=True, vmem_limit_bytes=60 * 1024 * 1024
-        ),
-    )(
+    operands = (
         residual,
         query_wide,
         key_wide,
@@ -936,6 +883,56 @@
         expert_up,
         expert_down,
     )
+    hbm = pl.BlockSpec(memory_space=pl.ANY)
+    dma = pltpu.SemaphoreType.DMA
+    return pl.pallas_call(
+        functools.partial(layer_kernel, n, groups, pieces, head_count // 2),
+        out_shape=jax.ShapeDtypeStruct((rows, width), bf),
+        in_specs=[hbm] * len(operands),
+        out_specs=hbm,
+        scratch_shapes=[pltpu.VMEM(a.shape, a.dtype) for a in operands[:-3]]
+        + [
+            pltpu.VMEM((n, 4 * head_count, rows), f32),
+            pltpu.VMEM((n,) + key_wide.shape, bf),
+            pltpu.VMEM((n,) + key_narrow.shape, bf),
+            pltpu.VMEM((n,) + values.shape, bf),
+            pltpu.VMEM((2, head_count, n, rows), f32),
+            pltpu.VMEM((2, head_count, rows, dv), f32),
+            pltpu.VMEM((2, head_count, rows, rows), f32),
+            pltpu.VMEM((n, cap, width), bf),
+            pltpu.VMEM((n_tp, n, cap, width), bf),
+            pltpu.VMEM((group_rows, n_tp * width), bf),
+            pltpu.VMEM((group_rows, expert_down.shape[1]), bf),
+            pltpu.VMEM((n_tp, groups, group_rows, width), bf),
+            pltpu.VMEM((2, groups, group_rows, width), bf),
+            pltpu.VMEM((groups, group_rows, width), bf),
+            pltpu.VMEM((groups, group_rows, width), bf),
+            pltpu.VMEM((groups, group_rows, width), bf),
+            pltpu.VMEM((n, cap, width), bf),
+            pltpu.VMEM(expert_gate.shape[1:], bf),
+            pltpu.VMEM(expert_up.shape[1:], bf),
+            pltpu.VMEM(expert_down.shape[1:], bf),
+            pltpu.VMEM((rows, width), bf),
+            dma((3,)),
+            dma((len(operands) - 3,)),
+            dma,
+            dma((n,)),
+            dma((n,)),
+            dma((3, 3, n)),
+            dma((3, n)),
+            dma((4, n)),
+            dma((4, n)),
+            dma((2, groups)),
+            dma((2, groups)),
+            dma((groups, pieces)),
+            dma((groups, pieces)),
+            dma((n,)),
+            dma((n,)),
+        ],
+        compiler_params=pltpu.CompilerParams(
+            collective_id=0, has_side_effects=True, vmem_limit_bytes=60 * 1024 * 1024
+        ),
+    )(*operands)
 
 
 def fits(n, n_tp, args):

time: 78.3 us -> 75.5 us (0.964)
  Pallas kernels: 76.5 us -> 73.8 us
    pallas_call x1, Pallas kernels: 76.5 us -> 73.8 us  [layer(): pl.pallas_call(functools.partial(layer_kernel, n, groups, pieces, head_co...]
where the time goes in v1:
time: 75.5 us; the launch traced here: 75.4 us
  Pallas kernels  73.8 us (98%)
  local copies, waits for them, and re-layouts  1.57 us (2%)
    pallas_call x1, Pallas kernels, layer(): pl.pallas_call(functools.partial(layer_kernel, n, groups, pieces, head_co...  73.8 us
    unnamed x1, local copies, waits for them, and re-layouts  1.57 us

profile of v1, /device:TPU:0, one launch (start us, length us, event | category | flops | bytes accessed | tf_op | source)
XLA Modules:
  0.0 75.4 jit_solution(8759191418973316940)
XLA Ops:
  0.0 73.8 %shard_map.136 = bf16[128,512]{1,0:T(8,128)(2,1)} custom-call(bf16[128,512]{1,0:T(8,128)(2,1)} %refs_0_.1, bf16[128,256]{1,0:T(8,128)(2,1)} %refs_1_.1, bf16[128,256]{1,0:T(8,128)(2,1)} %refs_2_.1, bf16[128,128]{1,0:T(8,128)(2,1)} %refs_3_.1, bf16[128,128]{1,0:T(8,128)(2,1)} %refs_4_.1, bf16[128,512]{1,0:T(8,128)(2,1)} %refs_5_.1, f32[8,128]{1,0:T(8,128)} %bitcast.6, ...), custom_call_target="tpu_custom_call" | custom-call | tf_op jit(solution)/shard_map/pallas_call | solution.py:888
  73.8 1.6 %copy.16 = bf16[128,512]{1,0:T(8,128)(2,1)} copy(bf16[128,512]{1,0:T(8,128)(2,1)} %shard_map.136) | data formatting | bytes 262144
